TPU v7x, 32 devices: a whole 2x2x4 slice. The times are simulated.
32 devices in a mesh: fs: 8 (over z, y), tp: 4 (over x, core).
Axes of the slice: x: 2, y: 2, z: 4, core: 2. Of those that a mesh axis runs over, the one named last changes fastest.
Arguments:
- tokens: bfloat16 [8, 384, 2048], P('fs', None, 'tp'), may hold values from -16 to 16
- first_gate: bfloat16 [2048, 6144], P('fs', 'tp'), may hold values from -0.125 to 0.125
- first_up: bfloat16 [2048, 6144], P('fs', 'tp'), may hold values from -0.125 to 0.125
- first_down: bfloat16 [6144, 2048], P('tp', 'fs'), may hold values from -0.078125 to 0.078125
- first_gain: bfloat16 [2048], P('tp'), may hold values from 0.099609375 to 1.8984375
- glu_value: bfloat16 [2048, 1024], P('fs', 'tp'), may hold values from -0.125 to 0.125
- glu_gate: bfloat16 [2048, 1024], P('fs', 'tp'), may hold values from -0.125 to 0.125
- conv_taps: bfloat16 [31, 1024], P(None, 'tp'), may hold values from -3 to 3
- conv_gain: bfloat16 [1024], P('tp'), may hold values from 0.099609375 to 1.8984375
- conv_proj: bfloat16 [1024, 2048], P('tp', 'fs'), may hold values from -0.1875 to 0.1875
- second_gain: bfloat16 [2048], P('tp'), may hold values from 0.099609375 to 1.8984375
- last_gate: bfloat16 [2048, 6144], P('fs', 'tp'), may hold values from -0.125 to 0.125
- last_up: bfloat16 [2048, 6144], P('fs', 'tp'), may hold values from -0.125 to 0.125
- last_down: bfloat16 [6144, 2048], P('tp', 'fs'), may hold values from -0.078125 to 0.078125
- third_gain: bfloat16 [2048], P('tp'), may hold values from 0.099609375 to 1.8984375
Outputs:
- layer_out: bfloat16 [8, 384, 2048], P('fs', None, 'tp')
All inputs are finite; a program needn't handle non-finite values.
Results may differ from a plain program's by a relative error of at most 0.015.
Values may be sent and summed in bfloat16 or wider, within the bound.
A program may use at most 64 MiB of HBM per device.

v0:
```python
import functools

import jax
import jax.numpy as jnp
from jax import lax
from jax.experimental import pallas as pl
from jax.experimental.pallas import tpu as pltpu
from jax.sharding import PartitionSpec as P

ALPHA = 2.0**0.25
EPSILON = 1e-05
MESH = pl.DeviceIdType.MESH
F32 = jnp.float32
BF16 = jnp.bfloat16


AHEAD_FIRST = 2
AHEAD_OWN = 1


def split_rows(rows, parts, step=16):
    swapped = max(step, (rows // 6 + step // 2) // step * step)
    units = (rows - swapped) // step
    sizes = [(units * (i + 1) // parts - units * i // parts) * step for i in range(parts)]
    return sizes, swapped


def plan_pieces(shapes, down, small, last):
    pieces = []
    for matrix, (rows, columns) in enumerate(shapes):
        if matrix in small:
            flip = matrix in down
            half = rows // 2
            pieces.append((matrix, 0, half, 0, columns, flip))
            pieces.append((matrix, half, half, 0, columns, False))
            continue
        wide = min(columns, 128) if matrix == last else columns
        for left in range(0, columns, wide):
            sizes, swapped = split_rows(rows, 2)
            order = [(sizes[0], False), (swapped, True)] + [(size, False) for size in sizes[1:]]
            start = 0
            for size, flip in order:
                pieces.append((matrix, start, size, left, wide, flip))
                start += size
    return pieces


def layer_kernel(
    n_fs,
    n_tp,
    n_y,
    pieces,
    tokens_ref,
    *refs,
):
    weights = refs[:9]
    first_gain, conv_taps, conv_gain, second_gain, third_gain = refs[9:14]
    out_ref = refs[14]
    bufs = refs[15:24]
    (xg, rs, send_buf, hidden, current, conv_in, acted, stat, z_s, z_r, y_s, y_r, loc_s, ag_s, ag_r, rs_s, rs_r, st_s, st_r, last_s, last_r) = refs[24:]

    n_z = n_fs // n_y
    fs = lax.axis_index("fs")
    tp = lax.axis_index("tp")
    z, y = fs // n_y, fs % n_y
    length, width = tokens_ref.shape
    features = width * n_tp

    barrier = pltpu.get_barrier_semaphore()
    for other in range(n_fs):
        @pl.when(other != fs)
        def _():
            pl.semaphore_signal(barrier, inc=1, device_id=(other, tp), device_id_type=MESH)
    for step in range(1, n_tp):
        pl.semaphore_signal(barrier, inc=1, device_id=(fs, (tp + step) % n_tp), device_id_type=MESH)
    pl.semaphore_wait(barrier, n_fs - 1 + n_tp - 1)

    pending = []

    def slot(c, block):
        matrix, start, size, left, wide, _ = pieces[c]
        buf = bufs[matrix]
        if len(buf.shape) == 2:
            rows = weights[matrix].shape[0]
            return buf.at[pl.ds(pl.multiple_of(block * rows + start, 16), size)]
        return buf.at[block, pl.ds(start, size), pl.ds(left, wide)]

    def own_rows(c):
        matrix, start, size, left, wide, _ = pieces[c]
        return weights[matrix].at[pl.ds(start, size), pl.ds(left, wide)]

    def remote(src, dst, s, r, dest):
        return pltpu.make_async_remote_copy(
            src_ref=src, dst_ref=dst, send_sem=s, recv_sem=r, device_id=dest, device_id_type=MESH
        )

    def axes(swapped):
        major, minor = (z, n_z, n_y), (y, n_y, 1)
        return (minor, major) if swapped else (major, minor)

    def when(cond, fn):
        pl.when(cond)(fn)

    def place(c, k, d, side):
        _, (_, extent, _) = axes(pieces[c][5])
        return (k * (extent - 1) + d - 1) * 2 + side

    def second_send(c, k, block, src):
        swapped = pieces[c][5]
        _, (pos, extent, stride) = axes(swapped)
        for side, sign in ((0, 1), (1, -1)):
            ok = pos < extent - 1 if side == 0 else pos > 0

            def go(side=side, sign=sign):
                i = place(c, k, 1, side)
                remote(src, slot(c, block), y_s.at[c, i], y_r.at[c, i], (fs + sign * stride, tp)).start()

            def done(side=side, sign=sign):
                i = place(c, k, 1, side)
                remote(src, slot(c, block), y_s.at[c, i], y_r.at[c, i], (fs + sign * stride, tp)).wait_send()

            when(ok, go)
            pending.append((ok, done))

    def own(c):
        swapped = pieces[c][5]
        src = own_rows(c)
        (pos, extent, stride), _ = axes(swapped)
        for side, sign in ((0, 1), (1, -1)):
            ok = pos < extent - 1 if side == 0 else pos > 0

            def copy(side=side, sign=sign):
                return remote(src, slot(c, fs), z_s.at[c, side], z_r.at[c, side], (fs + sign * stride, tp))

            when(ok, lambda copy=copy: copy().start())
            pending.append((ok, lambda copy=copy: copy().wait_send()))
        second_send(c, 0, fs, src)
        pltpu.make_async_copy(src, slot(c, fs), loc_s.at[c]).start()

    def first_axis(c):
        swapped = pieces[c][5]
        (pos, extent, stride), _ = axes(swapped)
        for d in range(1, extent):
            for side, sign in ((0, 1), (1, -1)):
                here = pos - sign * d >= 0 if side == 0 else pos + d < extent
                onward = here & (pos < extent - 1 if side == 0 else pos > 0)
                block = fs - sign * d * stride
                i = (d - 1) * 2 + side

                def arrive(block=block, i=i):
                    dst = slot(c, block)
                    remote(dst, dst, z_s.at[c, i], z_r.at[c, i], (fs, tp)).wait_recv()

                when(here, arrive)
                if d < extent - 1:
                    def copy(block=block, i=i, sign=sign):
                        dst = slot(c, block)
                        return remote(dst, dst, z_s.at[c, i + 2], z_r.at[c, i + 2], (fs + sign * stride, tp))

                    when(onward, lambda copy=copy: copy().start())
                    pending.append((onward, lambda copy=copy: copy().wait_send()))
                k = 1 + i
                _, (pos2, extent2, stride2) = axes(swapped)
                for side2, sign2 in ((0, 1), (1, -1)):
                    ok = here & (pos2 < extent2 - 1 if side2 == 0 else pos2 > 0)

                    def copy2(block=block, k=k, side2=side2, sign2=sign2, stride2=stride2):
                        j = place(c, k, 1, side2)
                        dst = slot(c, block)
                        return remote(dst, dst, y_s.at[c, j], y_r.at[c, j], (fs + sign2 * stride2, tp))

                    when(ok, lambda copy2=copy2: copy2().start())
                    pending.append((ok, lambda copy2=copy2: copy2().wait_send()))
                yield

    def second_axis(c):
        swapped = pieces[c][5]
        (pos, extent, stride), (pos2, extent2, stride2) = axes(swapped)
        origins = [(0, None, 0)] + [
            (1 + (d - 1) * 2 + side, side, d) for d in range(1, extent) for side in (0, 1)
        ]
        for d2 in range(1, extent2):
            for k, side, d in origins:
                if side is None:
                    here, first = True, fs
                else:
                    sign = 1 if side == 0 else -1
                    here = pos - d >= 0 if side == 0 else pos + d < extent
                    first = fs - sign * d * stride
                for side2, sign2 in ((0, 1), (1, -1)):
                    got = here & (pos2 - d2 >= 0 if side2 == 0 else pos2 + d2 < extent2)
                    block = first - sign2 * d2 * stride2
                    i = place(c, k, d2, side2)

                    def arrive(block=block, i=i):
                        dst = slot(c, block)
                        remote(dst, dst, y_s.at[c, i], y_r.at[c, i], (fs, tp)).wait_recv()

                    when(got, arrive)
                    if d2 < extent2 - 1:
                        ok = got & (pos2 < extent2 - 1 if side2 == 0 else pos2 > 0)

                        def copy(block=block, i=i, sign2=sign2):
                            dst = slot(c, block)
                            return remote(dst, dst, y_s.at[c, i + 2], y_r.at[c, i + 2], (fs + sign2 * stride2, tp))

                        when(ok, lambda copy=copy: copy().start())
                        pending.append((ok, lambda copy=copy: copy().wait_send()))
            yield
        pltpu.make_async_copy(own_rows(c), slot(c, fs), loc_s.at[c]).wait()

    landed = [0]

    def stream():
        count = len(pieces)
        lead = AHEAD_FIRST + AHEAD_OWN
        for c in range(min(lead, count)):
            own(c)
        yield
        for c in range(min(AHEAD_FIRST, count)):
            yield from first_axis(c)
        for c in range(count):
            if c + lead < count:
                own(c + lead)
            if c + AHEAD_FIRST < count:
                yield from first_axis(c + AHEAD_FIRST)
            yield from second_axis(c)
            landed[0] = c + 1
            yield

    pump_state = stream()

    def pump(steps):
        for _ in range(steps):
            next(pump_state, None)

    def until(matrix, right=None):
        need = 1 + max(
            i for i, piece in enumerate(pieces)
            if piece[0] == matrix and (right is None or piece[3] + piece[4] <= right)
        )
        while landed[0] < need:
            next(pump_state)

    def my_columns():
        return pl.ds(pl.multiple_of(tp * width, 128), width)

    def gather_start(phase, src):
        dst = xg.at[phase, :, my_columns()]
        for step in range(1, n_tp):
            i = step - 1
            remote(src, dst, ag_s.at[phase, i], ag_r.at[phase, i], (fs, (tp + step) % n_tp)).start()

    def gather_wait(phase, src):
        for step in range(1, n_tp):
            i = step - 1
            remote(src, src, ag_s.at[phase, i], ag_r.at[phase, i], (fs, tp)).wait()

    def scatter_start(phase):
        for step in range(1, n_tp):
            i = step - 1
            to = (tp + step) % n_tp
            remote(send_buf.at[to], rs.at[phase, i], rs_s.at[phase, i], rs_r.at[phase, i], (fs, to)).start()

    def scatter_columns(left, wide, part):
        copies = []
        n = left // wide
        for step in range(1, n_tp):
            i = step - 1
            to = (tp + step) % n_tp
            for q in range(width // part):
                cols = pl.ds(q * part + left, wide)
                j = (i * (part // wide) + n) * (width // part) + q
                copy = remote(
                    send_buf.at[to, :, cols], rs.at[2, i, :, cols], last_s.at[j], last_r.at[j], (fs, to)
                )
                copy.start()
                copies.append(copy)
        return copies

    def scatter_total(phase):
        total = send_buf[pl.ds(tp, 1)][0].astype(F32)
        for i in range(n_tp - 1):
            total = total + rs[phase, i].astype(F32)
        return total

    def scatter_wait(phase):
        for step in range(1, n_tp):
            i = step - 1
            remote(send_buf.at[0], rs.at[phase, i], rs_s.at[phase, i], rs_r.at[phase, i], (fs, tp)).wait()
        return scatter_total(phase)

    def stats_start(phase, values):
        sums = jnp.sum(values, axis=-1, keepdims=True)
        squares = jnp.sum(values * values, axis=-1, keepdims=True)
        lane = lax.broadcasted_iota(jnp.int32, (values.shape[0], 128), 1)
        both = jnp.where(lane == 0, sums, jnp.where(lane == 1, squares, 0.0))
        stat[phase, n_tp - 1] = both.T[:8]
        for step in range(1, n_tp):
            i = step - 1
            remote(
                stat.at[phase, n_tp - 1], stat.at[phase, i], st_s.at[phase, i], st_r.at[phase, i],
                (fs, (tp + step) % n_tp),
            ).start()

    def stats_wait(phase, all_width):
        for step in range(1, n_tp):
            i = step - 1
            remote(
                stat.at[phase, n_tp - 1], stat.at[phase, i], st_s.at[phase, i], st_r.at[phase, i], (fs, tp)
            ).wait()
        total = stat[phase, 0]
        for i in range(1, n_tp):
            total = total + stat[phase, i]
        both = jnp.concatenate([total] * 16, axis=0).T
        center = both[:, 0:1] / all_width
        spread = both[:, 1:2] / all_width - center * center
        return center, lax.rsqrt(spread + EPSILON)

    def ffn_hidden(phase, gate, up):
        tile = min(256, gate.shape[1])

        def step(j, carry):
            cols = pl.ds(pl.multiple_of(j * tile, 128), tile)
            held = xg[phase]
            g = jnp.dot(held, gate[:, cols], preferred_element_type=F32)
            u = jnp.dot(held, up[:, cols], preferred_element_type=F32)
            hidden[:, cols] = (g * jax.nn.sigmoid(g) * u).astype(BF16)
            return carry

        lax.fori_loop(0, gate.shape[1] // tile, step, 0)

    def project(source, buf, left=0, wide=None):
        part = buf.shape[2]
        per = width // part
        wide = wide or part

        def step(t, carry):
            held = source[...]
            for q in range(per):
                send_buf[t, :, q * part + left : q * part + left + wide] = jnp.dot(
                    held, buf[t * per + q, :, left : left + wide], preferred_element_type=F32
                ).astype(BF16)
            return carry

        lax.fori_loop(0, n_tp, step, 0)

    pump(1)
    xg[0, :, my_columns()] = tokens_ref[...]
    gather_start(0, tokens_ref)
    until(0)
    gather_wait(0, tokens_ref)
    until(1)
    ffn_hidden(0, bufs[0], bufs[1])
    until(2)
    project(hidden, bufs[2])
    scatter_start(0)
    pump(6)
    mixed = ALPHA * tokens_ref[...].astype(F32) + 0.5 * scatter_wait(0)
    current[...] = mixed
    stats_start(0, mixed)
    pump(4)
    center, scale = stats_wait(0, features)
    first = ((current[...] - center) * scale * first_gain[...].astype(F32)).astype(BF16)
    out_ref[...] = first
    xg[1, :, my_columns()] = first
    gather_start(1, out_ref)
    until(4)
    gather_wait(1, out_ref)

    channels = acted.shape[1]
    taps = conv_taps.shape[0]
    reach = (taps - 1) // 2
    margin = (conv_in.shape[0] - length) // 2
    held = xg[1]
    value = jnp.dot(held, bufs[3][...], preferred_element_type=F32)
    gate = jnp.dot(held, bufs[4][...], preferred_element_type=F32)
    conv_in[0:margin] = jnp.zeros((margin, channels), F32)
    conv_in[margin + length :] = jnp.zeros((margin, channels), F32)
    conv_in[margin : margin + length] = value * jax.nn.sigmoid(gate)
    pump(2)
    rows_each = length // 4
    for low in range(0, length, rows_each):
        for left in range(0, channels, 128):
            cols = slice(left, left + 128)
            total = jnp.zeros((rows_each, 128), F32)
            for tap in range(taps):
                start = margin - reach + low + tap
                total = total + conv_taps[tap : tap + 1, cols].astype(F32) * conv_in[start : start + rows_each, cols]
            current[low : low + rows_each, cols] = total
    stats_start(1, current[:, 0:channels])
    pump(4)
    center, scale = stats_wait(1, channels * n_tp)
    normed = (current[:, 0:channels] - center) * scale * conv_gain[...].astype(F32)
    acted[...] = (normed * jax.nn.sigmoid(normed)).astype(BF16)
    until(5)
    project(acted, bufs[5])
    scatter_start(1)
    pump(4)
    mixed = ALPHA * out_ref[...].astype(F32) + scatter_wait(1)
    current[...] = mixed
    stats_start(2, mixed)
    pump(4)
    center, scale = stats_wait(2, features)
    second = ((current[...] - center) * scale * second_gain[...].astype(F32)).astype(BF16)
    out_ref[...] = second
    xg[2, :, my_columns()] = second
    gather_start(2, out_ref)
    pump(4)
    gather_wait(2, out_ref)

    until(7)
    ffn_hidden(2, bufs[6], bufs[7])
    part = bufs[8].shape[2]
    wide = min(part, 128)
    copies = []
    for left in range(0, part, wide):
        until(8, left + wide)
        project(hidden, bufs[8], left, wide)
        copies += scatter_columns(left, wide, part)
    for _ in pump_state:
        pass
    for ok, done in pending:
        when(ok, done)
    for copy in copies:
        copy.wait()
    mixed = ALPHA * out_ref[...].astype(F32) + 0.5 * scatter_total(2)
    current[...] = mixed
    stats_start(3, mixed)
    center, scale = stats_wait(3, features)
    out_ref[...] = ((current[...] - center) * scale * third_gain[...].astype(F32)).astype(BF16)


def solution(mesh):
    n_fs, n_tp = mesh.shape["fs"], mesh.shape["tp"]
    n_y = 1 << ((n_fs.bit_length() - 1) // 2)
    if n_fs % n_y:
        n_y = 1

    def body(
        tokens, first_gate, first_up, first_down, first_gain, glu_value, glu_gate, conv_taps, conv_gain,
        conv_proj, second_gain, last_gate, last_up, last_down, third_gain,
    ):
        current = tokens[0]
        length, width = current.shape
        weights = (first_gate, first_up, first_down, glu_value, glu_gate, conv_proj, last_gate, last_up, last_down)
        down = (2, 5, 8)
        pieces = plan_pieces([w.shape for w in weights], down, (3, 4, 5), 8)
        n_z = n_fs // n_y
        first_slots = 2 * (max(n_z, n_y) - 1)
        second_slots = 2 * max(
            (1 + 2 * (n_z - 1)) * (n_y - 1),
            (1 + 2 * (n_y - 1)) * (n_z - 1),
        )
        channels = glu_value.shape[1]
        reach = (conv_taps.shape[0] - 1) // 2
        margin = -(-reach // 8) * 8
        n_last = (n_tp - 1) * (width // min(last_down.shape[1], 128))
        bufs = [
            pltpu.VMEM((n_fs,) + w.shape if i in down else (n_fs * w.shape[0], w.shape[1]), BF16)
            for i, w in enumerate(weights)
        ]
        dma = pltpu.SemaphoreType.DMA
        vmem = pl.BlockSpec(memory_space=pltpu.VMEM)
        result = pl.pallas_call(
            functools.partial(layer_kernel, n_fs, n_tp, n_y, pieces),
            out_shape=jax.ShapeDtypeStruct((length, width), BF16),
            in_specs=[vmem] + [pl.BlockSpec(memory_space=pl.ANY)] * 9 + [vmem] * 5,
            out_specs=vmem,
            scratch_shapes=bufs
            + [
                pltpu.VMEM((3, length, width * n_tp), BF16),
                pltpu.VMEM((3, n_tp - 1, length, width), BF16),
                pltpu.VMEM((n_tp, length, width), BF16),
                pltpu.VMEM((length, first_gate.shape[1]), BF16),
                pltpu.VMEM((length, width), F32),
                pltpu.VMEM((length + 2 * margin, channels), F32),
                pltpu.VMEM((length, channels), BF16),
                pltpu.VMEM((4, n_tp, 8, length), F32),
                dma((len(pieces), first_slots)),
                dma((len(pieces), first_slots)),
                dma((len(pieces), second_slots)),
                dma((len(pieces), second_slots)),
                dma((len(pieces),)),
                dma((3, n_tp - 1)),
                dma((3, n_tp - 1)),
                dma((3, n_tp - 1)),
                dma((3, n_tp - 1)),
                dma((4, n_tp - 1)),
                dma((4, n_tp - 1)),
                dma((n_last,)),
                dma((n_last,)),
            ],
            compiler_params=pltpu.CompilerParams(
                collective_id=0, has_side_effects=True, vmem_limit_bytes=67000000
            ),
        )(
            current, *weights, first_gain[None], conv_taps, conv_gain[None], second_gain[None], third_gain[None]
        )
        return result[None]

    weight = P("fs", "tp")
    return jax.shard_map(
        body,
        mesh=mesh,
        in_specs=(
            P("fs", None, "tp"), weight, weight, P("tp", "fs"), P("tp"), weight, weight, P(None, "tp"), P("tp"),
            P("tp", "fs"), P("tp"), weight, weight, P("tp", "fs"), P("tp"),
        ),
        out_specs=P("fs", None, "tp"),
        check_vma=False,
    )
```

profile of v0, /device:TPU:0, one launch (start us, length us, event | category | flops | bytes accessed | tf_op | source)
XLA Modules:
  0.0 443.9 jit_solution(13477865529092632044)
XLA Ops:
  0.0 0.0 copy-start.3
  0.0 0.7 copy-done.3
  0.7 0.0 copy-start
  0.7 0.6 broadcast_in_dim.16.refs_11_
  1.2 0.1 copy-done
  1.3 0.0 copy-start.1
  1.3 0.6 broadcast_in_dim.15.refs_9_
  1.9 0.1 copy-done.1
  2.0 0.0 copy-start.2
  2.0 0.6 broadcast_in_dim.17.refs_12_
  2.6 0.1 copy-done.2
  2.7 0.6 broadcast_in_dim.18.refs_13_
  3.3 438.9 %shard_map.145 = bf16[384,512]{1,0:T(8,128)(2,1)} custom-call(bf16[384,512]{1,0:T(8,128)(2,1)} %bitcast.3, bf16[256,1536]{1,0:T(8,128)(2,1)} %refs_0_.1, bf16[256,1536]{1,0:T(8,128)(2,1)} %refs_1_.1, bf16[1536,256]{1,0:T(8,128)(2,1)} %refs_2_.1, bf16[256,256]{1,0:T(8,128)(2,1)} %refs_3_.1, bf16[256,256]{1,0:T(8,128)(2,1)} %refs_4_.1, ...), custom_call_target="tpu_custom_call" | custom-call | tf_op jit(solution)/shard_map/pallas_call | solution.py:465
  442.2 1.8 copy.17
Async XLA Ops:
  0.0 0.7 copy-start.3
  0.7 0.7 copy-start
  1.3 0.7 copy-start.1
  2.0 0.7 copy-start.2
where the time goes:
time: 444 us
  Pallas kernels  439 us (99%)
  local copies, waits for them, and re-layouts  5.06 us (1%)
    pallas_call x1, Pallas kernels, body(): pl.pallas_call(functools.partial(layer_kernel, n_fs, n_tp, n_y, pieces),...  439 us

commit v1 on v0

v1 whole, which is shorter than its diff:
```python
import functools

import jax
import jax.numpy as jnp
from jax import lax
from jax.experimental import pallas as pl
from jax.experimental.pallas import tpu as pltpu
from jax.sharding import PartitionSpec as P

ALPHA = 2.0**0.25
EPSILON = 1e-05
MESH = pl.DeviceIdType.MESH
F32 = jnp.float32
BF16 = jnp.bfloat16

CORES = 2
FIRST = (0, 1, 2)
CONV = (3, 4, 5)
LAST = (6, 7, 8)
DOWN = (2, 5, 8)
LEAD = 2


def flip(value, k, size):
    bit = 1
    while bit < size:
        if k & bit:
            value = value + bit - 2 * bit * ((value // bit) % 2)
        bit *= 2
    return value


def layer_kernel(n_z, n_y, n_x, tokens_ref, *refs):
    weights = refs[:9]
    first_gain, conv_taps, conv_gain, second_gain, third_gain = refs[9:14]
    out_ref = refs[14]
    bufs = refs[15:24]
    (xg, xc, hidden, core_out, core_in, side_out, side_in, held, line_out, line_in,
     c_core_out, c_core_in, c_side_out, c_side_in, current, conv_in, acted, stat) = refs[24:42]
    (wz_s, wz_r, wy_s, wy_r, own_s, gz_s, gz_r, gx_s, gx_r, gc_s, gc_r,
     rc_s, rc_r, rx_s, rx_r, rz_s, rz_r, st_s, st_r) = refs[42:]

    n_tp = n_x * CORES
    fs = lax.axis_index("fs")
    tp = lax.axis_index("tp")
    z, y = fs // n_y, fs % n_y
    x, core = tp // CORES, tp % CORES
    length, width = tokens_ref.shape
    features = width * n_tp
    chunk = hidden.shape[2]
    partner = (fs, x * CORES + 1 - core)
    z_order = [flip(z, k, n_z) for k in range(n_z - 1, -1, -1)]

    barrier = pltpu.get_barrier_semaphore()
    for k in range(1, n_z):
        pl.semaphore_signal(barrier, inc=1, device_id=(flip(z, k, n_z) * n_y + y, tp), device_id_type=MESH)
    for o in range(1, n_y):
        pl.semaphore_signal(barrier, inc=1, device_id=(z * n_y + (y + o) % n_y, tp), device_id_type=MESH)
    for o in range(1, n_tp):
        pl.semaphore_signal(barrier, inc=1, device_id=(fs, (tp + o) % n_tp), device_id_type=MESH)
    pl.semaphore_wait(barrier, n_z - 1 + n_y - 1 + n_tp - 1)

    pending = {}

    def remote(src, dst, s, r, dest):
        return pltpu.make_async_remote_copy(
            src_ref=src, dst_ref=dst, send_sem=s, recv_sem=r, device_id=dest, device_id_type=MESH
        )

    def when(ok, fn):
        if ok is None:
            fn()
        else:
            pl.when(ok)(fn)

    def send(group, src, dst, s, r, dest, ok=None):
        when(ok, lambda: remote(src, dst, s, r, dest).start())
        pending.setdefault(group, []).append((ok, lambda: remote(src, dst, s, r, dest).wait_send()))

    def arrive(dst, s, r):
        remote(dst, dst, s, r, (fs, tp)).wait_recv()

    def flush(*groups):
        for group in groups:
            for ok, done in pending.pop(group, []):
                when(ok, done)

    def slot(m, block):
        if m in DOWN:
            return bufs[m].at[block]
        rows = bufs[m].shape[0] // (n_z * n_y)
        return bufs[m].at[pl.ds(pl.multiple_of(block * rows, 16), rows)]

    def part_of(m, zz):
        if m in CONV:
            return weights[m]
        if m in DOWN:
            return weights[m].at[pl.ds(pl.multiple_of(zz * chunk, 16), chunk)]
        if len(weights[m].shape) == 3:
            return weights[m].at[zz]
        return weights[m].at[:, pl.ds(pl.multiple_of(zz * chunk, 128), chunk)]

    def to_y(m, zz, src):
        for o in range(1, n_y):
            send(
                "weights", src, slot(m, zz * n_y + y), wy_s.at[m, zz, o - 1], wy_r.at[m, zz, o - 1],
                (z * n_y + (y + o) % n_y, tp),
            )

    def weight_send(m):
        if m in CONV:
            for side, sign in ((0, 1), (1, -1)):
                ok = z < n_z - 1 if side == 0 else z > 0
                send(
                    "weights", weights[m], slot(m, fs), wz_s.at[m, side], wz_r.at[m, side],
                    (fs + sign * n_y, tp), ok,
                )
        else:
            for k in range(n_z - 1, 0, -1):
                zz = flip(z, k, n_z)
                send("weights", part_of(m, zz), slot(m, fs), wz_s.at[m, k], wz_r.at[m, k], (zz * n_y + y, tp))
        own = part_of(m, z)
        to_y(m, z, own)
        pltpu.make_async_copy(own, slot(m, fs), own_s.at[m]).start()

    def weight_steps(m):
        for k in range(n_z - 1, 0, -1):
            if m in CONV:
                d = n_z - k
                for side, sign in ((0, 1), (1, -1)):
                    zz = z - sign * d
                    here = zz >= 0 if side == 0 else zz < n_z
                    onward = here & (z < n_z - 1 if side == 0 else z > 0)
                    i = (d - 1) * 2 + side
                    block = slot(m, zz * n_y + y)
                    when(here, lambda: arrive(block, wz_s.at[m, i], wz_r.at[m, i]))
                    if d < n_z - 1:
                        send(
                            "weights", block, block, wz_s.at[m, i + 2], wz_r.at[m, i + 2],
                            (fs + sign * n_y, tp), onward,
                        )
                    for o in range(1, n_y):
                        send(
                            "weights", block, block, wy_s.at[m, zz, o - 1], wy_r.at[m, zz, o - 1],
                            (z * n_y + (y + o) % n_y, tp), here,
                        )
            else:
                zz = flip(z, k, n_z)
                block = slot(m, zz * n_y + y)
                arrive(block, wz_s.at[m, k], wz_r.at[m, k])
                to_y(m, zz, block)
            yield

    def weight_ready(m):
        for k in range(n_z):
            zz = flip(z, k, n_z)
            for o in range(1, n_y):
                arrive(slot(m, zz * n_y + (y + n_y - o) % n_y), wy_s.at[m, zz, o - 1], wy_r.at[m, zz, o - 1])
        pltpu.make_async_copy(part_of(m, z), slot(m, fs), own_s.at[m]).wait()

    landed = [0]

    def stream():
        count = len(weights)
        for m in range(LEAD):
            weight_send(m)
        yield
        for m in range(count):
            if m + LEAD < count:
                weight_send(m + LEAD)
            for _ in weight_steps(m):
                yield
            landed[0] = m + 1

    stream_state = stream()

    def pump(steps):
        for _ in range(steps):
            next(stream_state, None)

    def until(*matrices):
        while landed[0] <= max(matrices):
            next(stream_state, None)
        for m in matrices:
            weight_ready(m)

    def columns(t):
        return pl.ds(pl.multiple_of(t * width, 128), width)

    def spread(group, src, dst, x_s, x_r, c_s, c_r, ok=None):
        for o in range(1, n_x):
            send(group, src, dst(tp), x_s(o - 1), x_r(o - 1), (fs, (x + o) % n_x * CORES + core), ok)
        send(group, src, dst(tp), c_s(x), c_r(x), partner, ok)

    def pass_on(group, dst, x_s, x_r, c_s, c_r, ok=None):
        for o in range(1, n_x):
            xx = (x + n_x - o) % n_x
            block = dst(xx * CORES + core)
            when(ok, lambda: arrive(block, x_s(o - 1), x_r(o - 1)))
            send(group, block, block, c_s(xx), c_r(xx), partner, ok)

    def collect(dst, c_s, c_r, ok=None):
        for o in range(n_x):
            xx = (x + o) % n_x
            when(ok, lambda: arrive(dst(xx * CORES + 1 - core), c_s(xx), c_r(xx)))

    def seq_refs(f, zz):
        return (
            lambda t: xg.at[f, zz, :, columns(t)],
            lambda i: gx_s.at[f, zz, i], lambda i: gx_r.at[f, zz, i],
            lambda i: gc_s.at[f, zz, i], lambda i: gc_r.at[f, zz, i],
        )

    def sides(d):
        for side, sign in ((0, 1), (1, -1)):
            zz = z - sign * d
            yield side, sign, zz, (zz >= 0 if side == 0 else zz < n_z)

    def gather(f, src, use=None):
        group = ("gather", f)
        for side, sign in ((0, 1), (1, -1)):
            ok = z < n_z - 1 if side == 0 else z > 0
            send(
                group, src, xg.at[f, z, :, columns(tp)], gz_s.at[f, side], gz_r.at[f, side],
                (fs + sign * n_y, tp), ok,
            )
        spread(group, src, *seq_refs(f, z))
        xg[f, z, :, columns(tp)] = src[...]
        yield
        for d in range(1, n_z + 1):
            if d < n_z:
                for side, sign, zz, here in sides(d):
                    onward = here & (z < n_z - 1 if side == 0 else z > 0)
                    i = (d - 1) * 2 + side
                    block = xg.at[f, zz, :, columns(tp)]
                    when(here, lambda: arrive(block, gz_s.at[f, i], gz_r.at[f, i]))
                    if d < n_z - 1:
                        send(
                            group, block, block, gz_s.at[f, i + 2], gz_r.at[f, i + 2],
                            (fs + sign * n_y, tp), onward,
                        )
                    spread(group, block, *seq_refs(f, zz), ok=here)
            yield
            if d == 1:
                pass_on(group, *seq_refs(f, z))
            else:
                for side, sign, zz, here in sides(d - 1):
                    pass_on(group, *seq_refs(f, zz), ok=here)
            yield
            if d == 1:
                dst, _, _, c_s, c_r = seq_refs(f, z)
                collect(dst, c_s, c_r)
                if use is not None:
                    use(z, None)
            else:
                for side, sign, zz, here in sides(d - 1):
                    dst, _, _, c_s, c_r = seq_refs(f, zz)
                    collect(dst, c_s, c_r, here)
                    if use is not None:
                        use(zz, here)

    def ffn_hidden(f, zz, gate, up):
        rows = xg[f, zz]
        g = jnp.dot(rows, gate[...], preferred_element_type=F32)
        u = jnp.dot(rows, up[...], preferred_element_type=F32)
        hidden[zz] = (g * jax.nn.sigmoid(g) * u).astype(BF16)

    def project(source, down, t):
        part = down.shape[2]
        per = width // part
        for q in range(per):
            yield slice(q * part, (q + 1) * part), jnp.dot(source[...], down[t * per + q], preferred_element_type=F32)

    def reduce_give(group, source, down, outgoing, incoming, s, r):
        for o in [*range(1, n_x), 0]:
            xx = (x + o) % n_x
            for cols, value in project(source, down, xx * CORES + 1 - core):
                outgoing(xx)[:, cols] = value.astype(BF16)
            send(group, outgoing(xx), incoming(xx), s(xx), r(xx), partner)

    def reduce_take(group, source, down, incoming, s, r, outgoing, target, xs, xr, keep):
        for o in [*range(1, n_x), 0]:
            xx = (x + o) % n_x
            arrive(incoming(xx), s(xx), r(xx))
            for cols, value in project(source, down, xx * CORES + core):
                total = value + incoming(xx)[:, cols].astype(F32)
                if o:
                    outgoing(o - 1)[:, cols] = total.astype(BF16)
                else:
                    keep[:, cols] = total
            if o:
                send(group, outgoing(o - 1), target(o - 1), xs(o - 1), xr(o - 1), (fs, xx * CORES + core))

    def reduce_sum(target, xs, xr, keep):
        total = keep[...]
        for o in range(1, n_x):
            arrive(target(o - 1), xs(o - 1), xr(o - 1))
            total = total + target(o - 1)[...].astype(F32)
        keep[...] = total

    def reduce_ffn(f, down, pumps):
        group = ("reduce", f)

        def give(zz):
            reduce_give(
                group, hidden.at[zz], down, lambda i: core_out.at[zz, i], lambda i: core_in.at[zz, i],
                lambda i: rc_s.at[f, zz, i], lambda i: rc_r.at[f, zz, i],
            )

        def take(zz):
            reduce_take(
                group, hidden.at[zz], down, lambda i: core_in.at[zz, i],
                lambda i: rc_s.at[f, zz, i], lambda i: rc_r.at[f, zz, i],
                lambda i: side_out.at[zz, i], lambda i: side_in.at[zz, i],
                lambda i: rx_s.at[f, zz, i], lambda i: rx_r.at[f, zz, i], held.at[zz],
            )

        give(z_order[0])
        for i in range(n_z):
            if i + 1 < n_z:
                give(z_order[i + 1])
            take(z_order[i])
        for i, zz in enumerate(z_order):
            pump(pumps)
            reduce_sum(
                lambda j: side_in.at[zz, j], lambda j: rx_s.at[f, zz, j], lambda j: rx_r.at[f, zz, j], held.at[zz]
            )
            own = i == n_z - 1
            for side, there in ((0, z > 0), (1, z < n_z - 1)):
                if not own:
                    there = there & (zz > z if side == 0 else zz < z)

                def add(side=side):
                    arrive(line_in.at[side, zz], rz_s.at[f, side, zz], rz_r.at[f, side, zz])
                    held[zz] = held[zz] + line_in[side, zz].astype(F32)

                when(there, add)
            if not own:
                line_out[zz] = held[zz].astype(BF16)
                for side, sign in ((0, 1), (1, -1)):
                    send(
                        group, line_out.at[zz], line_in.at[side, zz], rz_s.at[f, side, zz], rz_r.at[f, side, zz],
                        (fs + sign * n_y, tp), zz > z if side == 0 else zz < z,
                    )
        return held[z]

    def stats_start(phase, values):
        sums = jnp.sum(values, axis=-1, keepdims=True)
        squares = jnp.sum(values * values, axis=-1, keepdims=True)
        lane = lax.broadcasted_iota(jnp.int32, (values.shape[0], 128), 1)
        both = jnp.where(lane == 0, sums, jnp.where(lane == 1, squares, 0.0))
        stat[phase, n_tp - 1] = both.T[:8]
        for step in range(1, n_tp):
            i = step - 1
            remote(
                stat.at[phase, n_tp - 1], stat.at[phase, i], st_s.at[phase, i], st_r.at[phase, i],
                (fs, (tp + step) % n_tp),
            ).start()

    def stats_wait(phase, all_width):
        for step in range(1, n_tp):
            i = step - 1
            remote(
                stat.at[phase, n_tp - 1], stat.at[phase, i], st_s.at[phase, i], st_r.at[phase, i], (fs, tp)
            ).wait()
        total = stat[phase, 0]
        for i in range(1, n_tp):
            total = total + stat[phase, i]
        both = jnp.concatenate([total] * 16, axis=0).T
        center = both[:, 0:1] / all_width
        spread_of = both[:, 1:2] / all_width - center * center
        return center, lax.rsqrt(spread_of + EPSILON)

    def post_norm(phase, gain):
        stats_start(phase, current[...])
        pump(1)
        center, scale = stats_wait(phase, features)
        return ((current[...] - center) * scale * gain[...].astype(F32)).astype(BF16)

    steps = gather(0, tokens_ref)
    next(steps)
    pump(1)
    for _ in steps:
        pump(1)
    until(0, 1)
    lax.fori_loop(0, n_z, lambda i, c: (ffn_hidden(0, i, bufs[0], bufs[1]), c)[1], 0)
    until(2)
    current[...] = ALPHA * tokens_ref[...].astype(F32) + 0.5 * reduce_ffn(0, bufs[2], 1)
    first = post_norm(0, first_gain)
    out_ref[...] = first

    conv_refs = (
        lambda t: xc.at[:, columns(t)],
        lambda i: gx_s.at[2, 0, i], lambda i: gx_r.at[2, 0, i],
        lambda i: gc_s.at[2, 0, i], lambda i: gc_r.at[2, 0, i],
    )
    spread("conv", out_ref, *conv_refs)
    xc[:, columns(tp)] = first
    until(3, 4)
    pass_on("conv", *conv_refs)
    collect(conv_refs[0], conv_refs[3], conv_refs[4])

    channels = acted.shape[1]
    taps = conv_taps.shape[0]
    reach = (taps - 1) // 2
    margin = (conv_in.shape[0] - length) // 2
    rows = xc[...]
    value = jnp.dot(rows, bufs[3][...], preferred_element_type=F32)
    gate = jnp.dot(rows, bufs[4][...], preferred_element_type=F32)
    conv_in[0:margin] = jnp.zeros((margin, channels), F32)
    conv_in[margin + length :] = jnp.zeros((margin, channels), F32)
    conv_in[margin : margin + length] = value * jax.nn.sigmoid(gate)
    pump(1)
    rows_each = length // 4
    for low in range(0, length, rows_each):
        for left in range(0, channels, 128):
            cols = slice(left, left + 128)
            total = jnp.zeros((rows_each, 128), F32)
            for tap in range(taps):
                start = margin - reach + low + tap
                total = total + conv_taps[tap : tap + 1, cols].astype(F32) * conv_in[start : start + rows_each, cols]
            current[low : low + rows_each, cols] = total
    stats_start(1, current[:, 0:channels])
    pump(1)
    center, scale = stats_wait(1, channels * n_tp)
    normed = (current[:, 0:channels] - center) * scale * conv_gain[...].astype(F32)
    acted[...] = (normed * jax.nn.sigmoid(normed)).astype(BF16)
    until(5)
    conv_core = (
        lambda i: rc_s.at[2, 0, i], lambda i: rc_r.at[2, 0, i],
    )
    conv_side = (lambda i: rx_s.at[2, 0, i], lambda i: rx_r.at[2, 0, i])
    reduce_give("conv", acted, bufs[5], lambda i: c_core_out.at[i], lambda i: c_core_in.at[i], *conv_core)
    pump(1)
    reduce_take(
        "conv", acted, bufs[5], lambda i: c_core_in.at[i], *conv_core,
        lambda i: c_side_out.at[i], lambda i: c_side_in.at[i], *conv_side, current,
    )
    pump(2)
    reduce_sum(lambda i: c_side_in.at[i], *conv_side, current)
    current[...] = ALPHA * out_ref[...].astype(F32) + current[...]
    second = post_norm(2, second_gain)
    flush("conv")
    out_ref[...] = second

    steps = gather(1, out_ref)
    next(steps)
    until(6, 7)
    for _ in steps:
        pump(1)
    lax.fori_loop(0, n_z, lambda i, c: (ffn_hidden(1, i, bufs[6], bufs[7]), c)[1], 0)
    until(8)
    flush(("reduce", 0))
    current[...] = ALPHA * out_ref[...].astype(F32) + 0.5 * reduce_ffn(1, bufs[8], 1)
    pump(100)
    normed = post_norm(3, third_gain)
    flush("weights", ("gather", 0), ("gather", 1), ("reduce", 1))
    out_ref[...] = normed


def solution(mesh):
    n_fs, n_tp = mesh.shape["fs"], mesh.shape["tp"]
    n_y = 1 << ((n_fs.bit_length() - 1) // 2)
    n_z, n_x = n_fs // n_y, n_tp // CORES

    def body(
        tokens, first_gate, first_up, first_down, first_gain, glu_value, glu_gate, conv_taps, conv_gain,
        conv_proj, second_gain, last_gate, last_up, last_down, third_gain,
    ):
        tokens = tokens[0]
        length, width = tokens.shape
        features = width * n_tp
        chunk = first_gate.shape[1] // n_z

        def by_chunk(w):
            if chunk % 128 == 0:
                return w
            return jnp.swapaxes(w.reshape(w.shape[0], n_z, chunk), 0, 1)

        weights = (
            by_chunk(first_gate), by_chunk(first_up), first_down, glu_value, glu_gate, conv_proj,
            by_chunk(last_gate), by_chunk(last_up), last_down,
        )
        channels = glu_value.shape[1]
        reach = (conv_taps.shape[0] - 1) // 2
        margin = -(-reach // 8) * 8
        part = first_down.shape[1]
        wide = pltpu.VMEM((features, chunk), BF16)
        down = pltpu.VMEM((n_fs, chunk, part), BF16)
        glu = pltpu.VMEM((features, channels), BF16)
        proj = pltpu.VMEM((n_fs, channels, part), BF16)
        dma = pltpu.SemaphoreType.DMA
        vmem = pl.BlockSpec(memory_space=pltpu.VMEM)
        others = max(n_x - 1, 1)

        def blocks(*lead, kind=BF16):
            return pltpu.VMEM(lead + (length, width), kind)

        def pair(*shape):
            return [dma(shape), dma(shape)]

        result = pl.pallas_call(
            functools.partial(layer_kernel, n_z, n_y, n_x),
            out_shape=jax.ShapeDtypeStruct((length, width), BF16),
            in_specs=[vmem] + [pl.BlockSpec(memory_space=pl.ANY)] * 9 + [vmem] * 5,
            out_specs=vmem,
            scratch_shapes=[wide, wide, down, glu, glu, proj, wide, wide, down]
            + [
                pltpu.VMEM((2, n_z, length, features), BF16),
                pltpu.VMEM((length, features), BF16),
                pltpu.VMEM((n_z, length, chunk), BF16),
                blocks(n_z, n_x),
                blocks(n_z, n_x),
                blocks(n_z, others),
                blocks(n_z, others),
                blocks(n_z, kind=F32),
                blocks(n_z),
                blocks(2, n_z),
                blocks(n_x),
                blocks(n_x),
                blocks(others),
                blocks(others),
                blocks(kind=F32),
                pltpu.VMEM((length + 2 * margin, channels), F32),
                pltpu.VMEM((length, channels), BF16),
                pltpu.VMEM((4, n_tp, 8, length), F32),
            ]
            + pair(9, 2 * n_z)
            + pair(9, n_z, max(n_y - 1, 1))
            + [dma((9,))]
            + pair(2, 2 * n_z)
            + pair(3, n_z, others)
            + pair(3, n_z, n_x)
            + pair(3, n_z, n_x)
            + pair(3, n_z, others)
            + pair(2, 2, n_z)
            + pair(4, n_tp - 1),
            compiler_params=pltpu.CompilerParams(
                collective_id=0, has_side_effects=True, vmem_limit_bytes=67000000
            ),
        )(
            tokens, *weights, first_gain[None], conv_taps, conv_gain[None], second_gain[None], third_gain[None]
        )
        return result[None]

    weight = P("fs", "tp")
    return jax.shard_map(
        body,
        mesh=mesh,
        in_specs=(
            P("fs", None, "tp"), weight, weight, P("tp", "fs"), P("tp"), weight, weight, P(None, "tp"), P("tp"),
            P("tp", "fs"), P("tp"), weight, weight, P("tp", "fs"), P("tp"),
        ),
        out_specs=P("fs", None, "tp"),
        check_vma=False,
    )
```

time: 444 us -> 342 us (0.77)
  Pallas kernels: 439 us -> 337 us
    pallas_call x1, Pallas kernels: 439 us -> 337 us  [body(): pl.pallas_call(functools.partial(layer_kernel, n_z, n_y, n_x), out_shape=...]
where the time goes in v1:
time: 342 us
  Pallas kernels  337 us (99%)
  local copies, waits for them, and re-layouts  5.06 us (1%)
    pallas_call x1, Pallas kernels, body(): pl.pallas_call(functools.partial(layer_kernel, n_z, n_y, n_x), out_shape=...  337 us

profile of v1, /device:TPU:0, one launch (start us, length us, event | category | flops | bytes accessed | tf_op | source)
XLA Modules:
  0.0 341.8 jit_solution(3924036610990281572)
XLA Ops:
  0.0 0.0 copy-start.3
  0.0 0.7 copy-done.3
  0.7 0.0 copy-start
  0.7 0.6 broadcast_in_dim.16.refs_11_
  1.2 0.1 copy-done
  1.3 0.0 copy-start.1
  1.3 0.6 broadcast_in_dim.15.refs_9_
  1.9 0.1 copy-done.1
  2.0 0.0 copy-start.2
  2.0 0.6 broadcast_in_dim.17.refs_12_
  2.6 0.1 copy-done.2
  2.7 0.6 broadcast_in_dim.18.refs_13_
  3.3 336.7 %shard_map.145 = bf16[384,512]{1,0:T(8,128)(2,1)} custom-call(bf16[384,512]{1,0:T(8,128)(2,1)} %bitcast.3, bf16[256,1536]{1,0:T(8,128)(2,1)} %refs_0_.1, bf16[256,1536]{1,0:T(8,128)(2,1)} %refs_1_.1, bf16[1536,256]{1,0:T(8,128)(2,1)} %refs_2_.1, bf16[256,256]{1,0:T(8,128)(2,1)} %refs_3_.1, bf16[256,256]{1,0:T(8,128)(2,1)} %refs_4_.1, ...), custom_call_target="tpu_custom_call" | custom-call | tf_op jit(solution)/shard_map/pallas_call | solution.py:502
  340.0 1.8 copy.17
Async XLA Ops:
  0.0 0.7 copy-start.3
  0.7 0.7 copy-start
  1.3 0.7 copy-start.1
  2.0 0.7 copy-start.2

commit v2 on v1

v2 whole, which is shorter than its diff:
```python
import functools

import jax
import jax.numpy as jnp
from jax import lax
from jax.experimental import pallas as pl
from jax.experimental.pallas import tpu as pltpu
from jax.sharding import PartitionSpec as P

ALPHA = 2.0**0.25
EPSILON = 1e-05
MESH = pl.DeviceIdType.MESH
F32 = jnp.float32
BF16 = jnp.bfloat16

CORES = 2
FIRST = (0, 1, 2)
CONV = (3, 4, 5)
LAST = (6, 7, 8)
DOWN = (2, 5, 8)


def flip(value, k, size):
    bit = 1
    while bit < size:
        if k & bit:
            value = value + bit - 2 * bit * ((value // bit) % 2)
        bit *= 2
    return value


def low(k):
    return k & -k


def bits_below(limit):
    bit = 1
    while bit < limit:
        yield bit
        bit *= 2


def layer_kernel(n_z, n_y, n_x, cuts, tokens_ref, *refs):
    weights = refs[:9]
    first_gain, conv_taps, conv_gain, second_gain, third_gain = refs[9:14]
    out_ref = refs[14]
    bufs = refs[15:24]
    xgs, hiddens = refs[24:26], refs[26:28]
    (xc, core_out, core_in, side_out, side_in, held, line_out, line_in,
     c_core_out, c_core_in, c_side_out, c_side_in, current, conv_in, acted, stat) = refs[28:44]
    (wz_s, wz_r, wy_s, wy_r, own_s, gz_s, gz_r, gx_s, gx_r, gc_s, gc_r,
     rc_s, rc_r, rx_s, rx_r, rz_s, rz_r, st_s, st_r) = refs[44:]

    n_tp = n_x * CORES
    fs = lax.axis_index("fs")
    tp = lax.axis_index("tp")
    z, y = fs // n_y, fs % n_y
    x, core = tp // CORES, tp % CORES
    length, width = tokens_ref.shape
    features = width * n_tp
    partner = (fs, x * CORES + 1 - core)

    def along(k):
        return (flip(z, k, n_z) * n_y + y, tp)


    barrier = pltpu.get_barrier_semaphore()
    for k in range(1, n_z):
        pl.semaphore_signal(barrier, inc=1, device_id=(flip(z, k, n_z) * n_y + y, tp), device_id_type=MESH)
    for o in range(1, n_y):
        pl.semaphore_signal(barrier, inc=1, device_id=(z * n_y + (y + o) % n_y, tp), device_id_type=MESH)
    for o in range(1, n_tp):
        pl.semaphore_signal(barrier, inc=1, device_id=(fs, (tp + o) % n_tp), device_id_type=MESH)
    pl.semaphore_wait(barrier, n_z - 1 + n_y - 1 + n_tp - 1)

    pending = {}

    def remote(src, dst, s, r, dest):
        return pltpu.make_async_remote_copy(
            src_ref=src, dst_ref=dst, send_sem=s, recv_sem=r, device_id=dest, device_id_type=MESH
        )

    def send(group, src, dst, s, r, dest):
        copy = remote(src, dst, s, r, dest)
        copy.start()
        pending.setdefault(group, []).append(copy)

    def arrive(dst, s, r):
        remote(dst, dst, s, r, (fs, tp)).wait_recv()

    def flush(*groups):
        for group in groups:
            for copy in pending.pop(group, []):
                copy.wait_send()

    def slot(m, block):
        if m in DOWN:
            return bufs[m].at[block]
        rows = bufs[m].shape[0] // (n_z * n_y)
        return bufs[m].at[pl.ds(pl.multiple_of(block * rows, 16), rows)]

    def part_of(m, zz):
        if m in CONV:
            return weights[m]
        place = zz % cuts[m in LAST]
        chunk = hiddens[m in LAST].shape[2]
        if m in DOWN:
            return weights[m].at[pl.ds(pl.multiple_of(place * chunk, 16), chunk)]
        if len(weights[m].shape) == 3:
            return weights[m].at[place]
        return weights[m].at[:, pl.ds(pl.multiple_of(place * chunk, 128), chunk)]

    def to_y(m, k, src):
        for o in range(1, n_y):
            send(
                "weights", src, slot(m, along(k)[0]), wy_s.at[m, k, o - 1], wy_r.at[m, k, o - 1],
                (z * n_y + (y + o) % n_y, tp),
            )

    def tree_send(group, k, src, dst, s, r):
        for bit in bits_below(low(k) if k else n_z):
            send(group, src, dst, s(k ^ bit), r(k ^ bit), along(bit))

    def weight_own(*matrices):
        for m in matrices:
            own = part_of(m, z)
            to_y(m, 0, own)
            pltpu.make_async_copy(own, slot(m, fs), own_s.at[m]).start()

    def unit_send(m, k):
        zz = flip(z, k, n_z)
        send("weights", part_of(m, zz), slot(m, fs), wz_s.at[m, k], wz_r.at[m, k], along(k))

    def unit_forward(m, k):
        block = slot(m, along(k)[0])
        arrive(block, wz_s.at[m, k], wz_r.at[m, k])
        to_y(m, k, block)

    def conv_start():
        for m in CONV:
            tree_send("weights", 0, weights[m], slot(m, fs), lambda k: wz_s.at[m, k], lambda k: wz_r.at[m, k])
        weight_own(*CONV)

    def conv_block(k):
        for m in CONV:
            block = slot(m, along(k)[0])
            arrive(block, wz_s.at[m, k], wz_r.at[m, k])
            tree_send("weights", k, block, block, lambda i: wz_s.at[m, i], lambda i: wz_r.at[m, i])
            to_y(m, k, block)

    def weight_ready(m):
        for k in range(n_z):
            zz = flip(z, k, n_z)
            for o in range(1, n_y):
                arrive(slot(m, zz * n_y + (y + n_y - o) % n_y), wy_s.at[m, k, o - 1], wy_r.at[m, k, o - 1])
        pltpu.make_async_copy(part_of(m, z), slot(m, fs), own_s.at[m]).wait()

    units = [(m, k) for m in FIRST + LAST for k in range(n_z - 1, 0, -1)]
    sent, landed = [0], [0]

    def issue(count):
        for unit in units[sent[0] : sent[0] + count]:
            unit_send(*unit)
        sent[0] = min(sent[0] + count, len(units))

    def forward(count):
        for unit in units[landed[0] : landed[0] + count]:
            unit_forward(*unit)
        landed[0] = min(landed[0] + count, len(units))

    def until(*matrices):
        need = 1 + max((n for n, unit in enumerate(units) if unit[0] in matrices), default=-1)
        issue(max(need - sent[0], 0))
        forward(max(need - landed[0], 0))
        for m in matrices:
            weight_ready(m)

    def act(step):
        for fn, *args in step:
            fn(*args)

    def columns(t):
        return pl.ds(pl.multiple_of(t * width, 128), width)

    def spread(group, src, dst, x_s, x_r, c_s, c_r):
        for o in range(1, n_x):
            send(group, src, dst(tp), x_s(o - 1), x_r(o - 1), (fs, (x + o) % n_x * CORES + core))
        send(group, src, dst(tp), c_s(x), c_r(x), partner)

    def pass_on(group, dst, x_s, x_r, c_s, c_r):
        for o in range(1, n_x):
            xx = (x + n_x - o) % n_x
            block = dst(xx * CORES + core)
            arrive(block, x_s(o - 1), x_r(o - 1))
            send(group, block, block, c_s(xx), c_r(xx), partner)

    def collect(dst, x_s, x_r, c_s, c_r):
        for o in range(n_x):
            xx = (x + o) % n_x
            arrive(dst(xx * CORES + 1 - core), c_s(xx), c_r(xx))

    def seq_refs(f, k):
        return (
            lambda t: xgs[f].at[k, :, columns(t)],
            lambda i: gx_s.at[f, k, i], lambda i: gx_r.at[f, k, i],
            lambda i: gc_s.at[f, k, i], lambda i: gc_r.at[f, k, i],
        )

    def gather_start(f, src):
        group = ("gather", f)
        for bit in bits_below(cuts[f]):
            send(group, src, xgs[f].at[bit, :, columns(tp)], gz_s.at[f, bit], gz_r.at[f, bit], along(bit))
        spread(group, src, *seq_refs(f, 0))
        xgs[f][0, :, columns(tp)] = src[...]

    def gather_block(f, k):
        group = ("gather", f)
        block = xgs[f].at[k, :, columns(tp)]
        arrive(block, gz_s.at[f, k], gz_r.at[f, k])
        for bit in bits_below(low(k)):
            send(group, block, xgs[f].at[k ^ bit, :, columns(tp)], gz_s.at[f, k ^ bit], gz_r.at[f, k ^ bit], along(bit))
        spread(group, block, *seq_refs(f, k))

    def gather_pass(f, k):
        pass_on(("gather", f), *seq_refs(f, k))

    def ffn_hidden(f, k, gate, up):
        rows = xgs[f][k]
        g = jnp.dot(rows, gate[...], preferred_element_type=F32)
        u = jnp.dot(rows, up[...], preferred_element_type=F32)
        hiddens[f][k] = (g * jax.nn.sigmoid(g) * u).astype(BF16)

    def project(source, down, t):
        part = down.shape[2]
        per = width // part
        for q in range(per):
            yield slice(q * part, (q + 1) * part), jnp.dot(source[...], down[t * per + q], preferred_element_type=F32)

    def reduce_give(group, source, down, outgoing, incoming, s, r):
        for o in [*range(1, n_x), 0]:
            xx = (x + o) % n_x
            for cols, value in project(source, down, xx * CORES + 1 - core):
                outgoing(xx)[:, cols] = value.astype(BF16)
            send(group, outgoing(xx), incoming(xx), s(xx), r(xx), partner)

    def reduce_take(group, source, down, incoming, s, r, outgoing, target, xs, xr, keep):
        for o in [*range(1, n_x), 0]:
            xx = (x + o) % n_x
            arrive(incoming(xx), s(xx), r(xx))
            for cols, value in project(source, down, xx * CORES + core):
                total = value + incoming(xx)[:, cols].astype(F32)
                if o:
                    outgoing(o - 1)[:, cols] = total.astype(BF16)
                else:
                    keep[:, cols] = total
            if o:
                send(group, outgoing(o - 1), target(o - 1), xs(o - 1), xr(o - 1), (fs, xx * CORES + core))

    def reduce_sum(target, xs, xr, keep):
        total = keep[...]
        for o in range(1, n_x):
            arrive(target(o - 1), xs(o - 1), xr(o - 1))
            total = total + target(o - 1)[...].astype(F32)
        keep[...] = total

    def reduce_ffn(f, down, plan):
        group = ("reduce", f)

        def give(k):
            reduce_give(
                group, hiddens[f].at[k], down, lambda i: core_out.at[k, i], lambda i: core_in.at[k, i],
                lambda i: rc_s.at[f, k, i], lambda i: rc_r.at[f, k, i],
            )

        def take(k):
            reduce_take(
                group, hiddens[f].at[k], down, lambda i: core_in.at[k, i],
                lambda i: rc_s.at[f, k, i], lambda i: rc_r.at[f, k, i],
                lambda i: side_out.at[k, i], lambda i: side_in.at[k, i],
                lambda i: rx_s.at[f, k, i], lambda i: rx_r.at[f, k, i], held.at[k],
            )

        give(cuts[f] - 1)
        for k in range(cuts[f] - 1, -1, -1):
            if k:
                give(k - 1)
            take(k)
        act(plan.get("given", ()))
        for k in range(cuts[f] - 1, -1, -1):
            act(plan.get(k, ()))
            reduce_sum(
                lambda i: side_in.at[k, i], lambda i: rx_s.at[f, k, i], lambda i: rx_r.at[f, k, i], held.at[k]
            )
            total = held[k]
            for bit in bits_below(low(k) if k else cuts[f]):
                i = (k ^ bit) - 1
                arrive(line_in.at[i], rz_s.at[f, i], rz_r.at[f, i])
                total = total + line_in[i].astype(F32)
            if k == 0:
                return total
            line_out[k - 1] = total.astype(BF16)
            send(group, line_out.at[k - 1], line_in.at[k - 1], rz_s.at[f, k - 1], rz_r.at[f, k - 1], along(low(k)))

    def stats_start(phase, values):
        sums = jnp.sum(values, axis=-1, keepdims=True)
        squares = jnp.sum(values * values, axis=-1, keepdims=True)
        lane = lax.broadcasted_iota(jnp.int32, (values.shape[0], 128), 1)
        both = jnp.where(lane == 0, sums, jnp.where(lane == 1, squares, 0.0))
        stat[phase, n_tp - 1] = both.T[:8]
        for step in range(1, n_tp):
            i = step - 1
            remote(
                stat.at[phase, n_tp - 1], stat.at[phase, i], st_s.at[phase, i], st_r.at[phase, i],
                (fs, (tp + step) % n_tp),
            ).start()

    def stats_wait(phase, all_width):
        for step in range(1, n_tp):
            i = step - 1
            remote(
                stat.at[phase, n_tp - 1], stat.at[phase, i], st_s.at[phase, i], st_r.at[phase, i], (fs, tp)
            ).wait()
        total = stat[phase, 0]
        for i in range(1, n_tp):
            total = total + stat[phase, i]
        both = jnp.concatenate([total] * 16, axis=0).T
        center = both[:, 0:1] / all_width
        spread_of = both[:, 1:2] / all_width - center * center
        return center, lax.rsqrt(spread_of + EPSILON)

    def post_norm(phase, gain):
        stats_start(phase, current[...])
        center, scale = stats_wait(phase, features)
        return ((current[...] - center) * scale * gain[...].astype(F32)).astype(BF16)

    gather_start(0, tokens_ref)
    weight_own(*FIRST)
    issue(3)
    gather_block(0, 1)
    issue(1)
    gather_block(0, 2)
    issue(2)
    gather_pass(0, 0)
    forward(2)
    gather_block(0, 3)
    issue(3)
    conv_start()
    issue(1)
    gather_pass(0, 1)
    forward(1)
    gather_pass(0, 2)
    forward(1)
    gather_pass(0, 3)
    for k in range(n_z):
        collect(*seq_refs(0, k))
    until(0, 1)
    lax.fori_loop(0, n_z, lambda i, c: (ffn_hidden(0, i, bufs[0], bufs[1]), c)[1], 0)
    until(2)
    weight_own(LAST[0])
    current[...] = ALPHA * tokens_ref[...].astype(F32) + 0.5 * reduce_ffn(0, bufs[2], {
        "given": [(conv_block, 1), (conv_block, 2), (issue, 1)],
        2: [(forward, 1), (issue, 1)],
        1: [(forward, 1), (weight_own, LAST[1]), (issue, 1)],
        0: [(weight_own, LAST[2]), (issue, 1)],
    })
    first = post_norm(0, first_gain)
    out_ref[...] = first

    conv_refs = (
        lambda t: xc.at[:, columns(t)],
        lambda i: gx_s.at[2, 0, i], lambda i: gx_r.at[2, 0, i],
        lambda i: gc_s.at[2, 0, i], lambda i: gc_r.at[2, 0, i],
    )
    spread("conv", out_ref, *conv_refs)
    issue(1)
    xc[:, columns(tp)] = first
    conv_block(3)
    forward(2)
    pass_on("conv", *conv_refs)
    until(3, 4)
    collect(*conv_refs)

    channels = acted.shape[1]
    taps = conv_taps.shape[0]
    reach = (taps - 1) // 2
    margin = (conv_in.shape[0] - length) // 2
    rows = xc[...]
    value = jnp.dot(rows, bufs[3][...], preferred_element_type=F32)
    gate = jnp.dot(rows, bufs[4][...], preferred_element_type=F32)
    conv_in[0:margin] = jnp.zeros((margin, channels), F32)
    conv_in[margin + length :] = jnp.zeros((margin, channels), F32)
    conv_in[margin : margin + length] = value * jax.nn.sigmoid(gate)
    issue(2)
    forward(1)
    rows_each = length // 4
    for top in range(0, length, rows_each):
        for left in range(0, channels, 128):
            cols = slice(left, left + 128)
            total = jnp.zeros((rows_each, 128), F32)
            for tap in range(taps):
                start = margin - reach + top + tap
                total = total + conv_taps[tap : tap + 1, cols].astype(F32) * conv_in[start : start + rows_each, cols]
            current[top : top + rows_each, cols] = total
    stats_start(1, current[:, 0:channels])
    center, scale = stats_wait(1, channels * n_tp)
    normed = (current[:, 0:channels] - center) * scale * conv_gain[...].astype(F32)
    acted[...] = (normed * jax.nn.sigmoid(normed)).astype(BF16)
    until(5)
    conv_core = (lambda i: rc_s.at[2, 0, i], lambda i: rc_r.at[2, 0, i])
    conv_side = (lambda i: rx_s.at[2, 0, i], lambda i: rx_r.at[2, 0, i])
    reduce_give("conv", acted, bufs[5], lambda i: c_core_out.at[i], lambda i: c_core_in.at[i], *conv_core)
    issue(1)
    forward(1)
    reduce_take(
        "conv", acted, bufs[5], lambda i: c_core_in.at[i], *conv_core,
        lambda i: c_side_out.at[i], lambda i: c_side_in.at[i], *conv_side, current,
    )
    forward(1)
    reduce_sum(lambda i: c_side_in.at[i], *conv_side, current)
    current[...] = ALPHA * out_ref[...].astype(F32) + current[...]
    second = post_norm(2, second_gain)
    flush("conv")
    out_ref[...] = second

    gather_start(1, out_ref)
    forward(1)
    gather_block(1, 1)
    forward(1)
    gather_pass(1, 0)
    until(6, 7)
    collect(*seq_refs(1, 0))
    ffn_hidden(1, 0, bufs[6], bufs[7])
    for k in range(1, cuts[1]):
        if k > 1:
            gather_block(1, k)
        gather_pass(1, k)
        collect(*seq_refs(1, k))
        ffn_hidden(1, k, bufs[6], bufs[7])
    until(8)
    flush(("reduce", 0))
    current[...] = ALPHA * out_ref[...].astype(F32) + 0.5 * reduce_ffn(1, bufs[8], {})
    normed = post_norm(3, third_gain)
    flush("weights", ("gather", 0), ("gather", 1), ("reduce", 1))
    out_ref[...] = normed


def solution(mesh):
    n_fs, n_tp = mesh.shape["fs"], mesh.shape["tp"]
    n_y = 1 << ((n_fs.bit_length() - 1) // 2)
    n_z, n_x = n_fs // n_y, n_tp // CORES

    def body(
        tokens, first_gate, first_up, first_down, first_gain, glu_value, glu_gate, conv_taps, conv_gain,
        conv_proj, second_gain, last_gate, last_up, last_down, third_gain,
    ):
        tokens = tokens[0]
        length, width = tokens.shape
        features = width * n_tp
        cuts = (n_z, min(n_z, 2))
        chunks = [first_gate.shape[1] // cut for cut in cuts]

        def by_chunk(w, f):
            if chunks[f] % 128 == 0:
                return w
            return jnp.swapaxes(w.reshape(w.shape[0], cuts[f], chunks[f]), 0, 1)

        weights = (
            by_chunk(first_gate, 0), by_chunk(first_up, 0), first_down, glu_value, glu_gate, conv_proj,
            by_chunk(last_gate, 1), by_chunk(last_up, 1), last_down,
        )
        channels = glu_value.shape[1]
        reach = (conv_taps.shape[0] - 1) // 2
        margin = -(-reach // 8) * 8
        part = first_down.shape[1]
        wide = [pltpu.VMEM((features, chunk), BF16) for chunk in chunks]
        down = [pltpu.VMEM((n_fs, chunk, part), BF16) for chunk in chunks]
        glu = pltpu.VMEM((features, channels), BF16)
        proj = pltpu.VMEM((n_fs, channels, part), BF16)
        dma = pltpu.SemaphoreType.DMA
        vmem = pl.BlockSpec(memory_space=pltpu.VMEM)
        others, others_z = max(n_x - 1, 1), max(n_z - 1, 1)

        def blocks(*lead, kind=BF16):
            return pltpu.VMEM(lead + (length, width), kind)

        def pair(*shape):
            return [dma(shape), dma(shape)]

        result = pl.pallas_call(
            functools.partial(layer_kernel, n_z, n_y, n_x, cuts),
            out_shape=jax.ShapeDtypeStruct((length, width), BF16),
            in_specs=[vmem] + [pl.BlockSpec(memory_space=pl.ANY)] * 9 + [vmem] * 5,
            out_specs=vmem,
            scratch_shapes=[wide[0], wide[0], down[0], glu, glu, proj, wide[1], wide[1], down[1]]
            + [pltpu.VMEM((cut, length, features), BF16) for cut in cuts]
            + [pltpu.VMEM((cut, length, chunk), BF16) for cut, chunk in zip(cuts, chunks)]
            + [
                pltpu.VMEM((length, features), BF16),
                blocks(n_z, n_x),
                blocks(n_z, n_x),
                blocks(n_z, others),
                blocks(n_z, others),
                blocks(n_z, kind=F32),
                blocks(others_z),
                blocks(others_z),
                blocks(n_x),
                blocks(n_x),
                blocks(others),
                blocks(others),
                blocks(kind=F32),
                pltpu.VMEM((length + 2 * margin, channels), F32),
                pltpu.VMEM((length, channels), BF16),
                pltpu.VMEM((4, n_tp, 8, length), F32),
            ]
            + pair(9, n_z)
            + pair(9, n_z, max(n_y - 1, 1))
            + [dma((9,))]
            + pair(2, n_z)
            + pair(3, n_z, others)
            + pair(3, n_z, n_x)
            + pair(3, n_z, n_x)
            + pair(3, n_z, others)
            + pair(2, others_z)
            + pair(4, n_tp - 1),
            compiler_params=pltpu.CompilerParams(
                collective_id=0, has_side_effects=True, vmem_limit_bytes=67000000
            ),
        )(
            tokens, *weights, first_gain[None], conv_taps, conv_gain[None], second_gain[None], third_gain[None]
        )
        return result[None]

    weight = P("fs", "tp")
    return jax.shard_map(
        body,
        mesh=mesh,
        in_specs=(
            P("fs", None, "tp"), weight, weight, P("tp", "fs"), P("tp"), weight, weight, P(None, "tp"), P("tp"),
            P("tp", "fs"), P("tp"), weight, weight, P("tp", "fs"), P("tp"),
        ),
        out_specs=P("fs", None, "tp"),
        check_vma=False,
    )
```

time: 342 us -> 280 us (0.82); the launches traced: 342 us -> 276 us
  Pallas kernels: 337 us -> 271 us
    pallas_call x1, Pallas kernels: 337 us -> 271 us  [body(): pl.pallas_call(functools.partial(layer_kernel, n_z, n_y, n_x, cuts), out_...]
where the time goes in v2:
time: 280 us; the launch traced here: 276 us
  Pallas kernels  271 us (97%)
  local copies, waits for them, and re-layouts  5.06 us (2%)
    pallas_call x1, Pallas kernels, body(): pl.pallas_call(functools.partial(layer_kernel, n_z, n_y, n_x, cuts), out_...  271 us

profile of v2, /device:TPU:0, one launch (start us, length us, event | category | flops | bytes accessed | tf_op | source)
XLA Modules:
  0.0 276.2 jit_solution(12611586836946898724)
XLA Ops:
  0.0 0.0 copy-start.3
  0.0 0.7 copy-done.3
  0.7 0.0 copy-start
  0.7 0.6 broadcast_in_dim.16.refs_11_
  1.2 0.1 copy-done
  1.3 0.0 copy-start.1
  1.3 0.6 broadcast_in_dim.15.refs_9_
  1.9 0.1 copy-done.1
  2.0 0.0 copy-start.2
  2.0 0.6 broadcast_in_dim.17.refs_12_
  2.6 0.1 copy-done.2
  2.7 0.6 broadcast_in_dim.18.refs_13_
  3.3 271.1 %shard_map.145 = bf16[384,512]{1,0:T(8,128)(2,1)} custom-call(bf16[384,512]{1,0:T(8,128)(2,1)} %bitcast.3, bf16[256,1536]{1,0:T(8,128)(2,1)} %refs_0_.1, bf16[256,1536]{1,0:T(8,128)(2,1)} %refs_1_.1, bf16[1536,256]{1,0:T(8,128)(2,1)} %refs_2_.1, bf16[256,256]{1,0:T(8,128)(2,1)} %refs_3_.1, bf16[256,256]{1,0:T(8,128)(2,1)} %refs_4_.1, ...), custom_call_target="tpu_custom_call" | custom-call | tf_op jit(solution)/shard_map/pallas_call | solution.py:489
  274.4 1.8 copy.17
Async XLA Ops:
  0.0 0.7 copy-start.3
  0.7 0.7 copy-start
  1.3 0.7 copy-start.1
  2.0 0.7 copy-start.2

commit v3 on v2

--- a/solution.py
+++ b/solution.py
@@ -155,7 +155,8 @@
                 arrive(slot(m, zz * n_y + (y + n_y - o) % n_y), wy_s.at[m, k, o - 1], wy_r.at[m, k, o - 1])
         pltpu.make_async_copy(part_of(m, z), slot(m, fs), own_s.at[m]).wait()
 
-    units = [(m, k) for m in FIRST + LAST for k in range(n_z - 1, 0, -1)]
+    units = [(m, k) for m in FIRST for k in range(n_z - 1, 0, -1)]
+    units += [(m, k) for m in LAST for k in (1, *range(n_z - 1, 1, -1))]
     sent, landed = [0], [0]
 
     def issue(count):
@@ -328,13 +329,16 @@
         spread_of = both[:, 1:2] / all_width - center * center
         return center, lax.rsqrt(spread_of + EPSILON)
 
+    def row_of(gain):
+        return gain[...].astype(F32).reshape(1, gain.shape[0])
+
     def post_norm(phase, gain):
         stats_start(phase, current[...])
         center, scale = stats_wait(phase, features)
-        return ((current[...] - center) * scale * gain[...].astype(F32)).astype(BF16)
+        return ((current[...] - center) * scale * row_of(gain)).astype(BF16)
 
     gather_start(0, tokens_ref)
-    weight_own(*FIRST)
+    weight_own(*FIRST, *LAST[:2])
     issue(3)
     gather_block(0, 1)
     issue(1)
@@ -345,7 +349,7 @@
     gather_block(0, 3)
     issue(3)
     conv_start()
-    issue(1)
+    issue(2)
     gather_pass(0, 1)
     forward(1)
     gather_pass(0, 2)
@@ -354,15 +358,18 @@
     for k in range(n_z):
         collect(*seq_refs(0, k))
     until(0, 1)
-    lax.fori_loop(0, n_z, lambda i, c: (ffn_hidden(0, i, bufs[0], bufs[1]), c)[1], 0)
+    forward(2)
+    for low_k, high_k in ((0, n_z // 2), (n_z // 2, n_z)):
+        lax.fori_loop(low_k, high_k, lambda i, c: (ffn_hidden(0, i, bufs[0], bufs[1]), c)[1], 0)
+        forward(1 if low_k == 0 else 0)
     until(2)
-    weight_own(LAST[0])
     current[...] = ALPHA * tokens_ref[...].astype(F32) + 0.5 * reduce_ffn(0, bufs[2], {
         "given": [(conv_block, 1), (conv_block, 2), (issue, 1)],
-        2: [(forward, 1), (issue, 1)],
-        1: [(forward, 1), (weight_own, LAST[1]), (issue, 1)],
-        0: [(weight_own, LAST[2]), (issue, 1)],
+        2: [(forward, 1)],
+        1: [(forward, 1), (weight_own, LAST[2])],
     })
+    issue(2)
+    forward(1)
     first = post_norm(0, first_gain)
     out_ref[...] = first
 
@@ -372,10 +379,10 @@
         lambda i: gc_s.at[2, 0, i], lambda i: gc_r.at[2, 0, i],
     )
     spread("conv", out_ref, *conv_refs)
-    issue(1)
     xc[:, columns(tp)] = first
     conv_block(3)
-    forward(2)
+    forward(1)
+    issue(1)
     pass_on("conv", *conv_refs)
     until(3, 4)
     collect(*conv_refs)
@@ -390,8 +397,6 @@
     conv_in[0:margin] = jnp.zeros((margin, channels), F32)
     conv_in[margin + length :] = jnp.zeros((margin, channels), F32)
     conv_in[margin : margin + length] = value * jax.nn.sigmoid(gate)
-    issue(2)
-    forward(1)
     rows_each = length // 4
     for top in range(0, length, rows_each):
         for left in range(0, channels, 128):
@@ -403,14 +408,13 @@
             current[top : top + rows_each, cols] = total
     stats_start(1, current[:, 0:channels])
     center, scale = stats_wait(1, channels * n_tp)
-    normed = (current[:, 0:channels] - center) * scale * conv_gain[...].astype(F32)
+    normed = (current[:, 0:channels] - center) * scale * row_of(conv_gain)
     acted[...] = (normed * jax.nn.sigmoid(normed)).astype(BF16)
     until(5)
     conv_core = (lambda i: rc_s.at[2, 0, i], lambda i: rc_r.at[2, 0, i])
     conv_side = (lambda i: rx_s.at[2, 0, i], lambda i: rx_r.at[2, 0, i])
     reduce_give("conv", acted, bufs[5], lambda i: c_core_out.at[i], lambda i: c_core_in.at[i], *conv_core)
-    issue(1)
-    forward(1)
+    issue(2)
     reduce_take(
         "conv", acted, bufs[5], lambda i: c_core_in.at[i], *conv_core,
         lambda i: c_side_out.at[i], lambda i: c_side_in.at[i], *conv_side, current,
@@ -423,13 +427,15 @@
     out_ref[...] = second
 
     gather_start(1, out_ref)
-    forward(1)
+    issue(1)
+    forward(2)
     gather_block(1, 1)
     forward(1)
     gather_pass(1, 0)
     until(6, 7)
     collect(*seq_refs(1, 0))
     ffn_hidden(1, 0, bufs[6], bufs[7])
+    forward(1)
     for k in range(1, cuts[1]):
         if k > 1:
             gather_block(1, k)
@@ -526,7 +532,7 @@
                 collective_id=0, has_side_effects=True, vmem_limit_bytes=67000000
             ),
         )(
-            tokens, *weights, first_gain[None], conv_taps, conv_gain[None], second_gain[None], third_gain[None]
+            tokens, *weights, first_gain, conv_taps, conv_gain, second_gain, third_gain
         )
         return result[None]
 

time: 280 us -> 260 us (0.929); the launches traced: 276 us -> 260 us
  Pallas kernels: 271 us -> 258 us
  local copies, waits for them, and re-layouts: 5.06 us -> 1.77 us
    pallas_call x1, Pallas kernels: 271 us -> 258 us  [body(): pl.pallas_call(functools.partial(layer_kernel, n_z, n_y, n_x, cuts), out_...]
where the time goes in v3:
time: 260 us
  Pallas kernels  258 us (99%)
    pallas_call x1, Pallas kernels, body(): pl.pallas_call(functools.partial(layer_kernel, n_z, n_y, n_x, cuts), out_...  258 us

profile of v3, /device:TPU:0, one launch (start us, length us, event | category | flops | bytes accessed | tf_op | source)
XLA Modules:
  0.0 260.1 jit_solution(8653860071146293336)
XLA Ops:
  0.0 258.3 %shard_map.145 = bf16[384,512]{1,0:T(8,128)(2,1)} custom-call(bf16[384,512]{1,0:T(8,128)(2,1)} %bitcast.3, bf16[256,1536]{1,0:T(8,128)(2,1)} %refs_0_.1, bf16[256,1536]{1,0:T(8,128)(2,1)} %refs_1_.1, bf16[1536,256]{1,0:T(8,128)(2,1)} %refs_2_.1, bf16[256,256]{1,0:T(8,128)(2,1)} %refs_3_.1, bf16[256,256]{1,0:T(8,128)(2,1)} %refs_4_.1, ...), custom_call_target="tpu_custom_call" | custom-call | tf_op jit(solution)/shard_map/pallas_call | solution.py:495
  258.3 1.8 copy.17

commit v4 on v3

--- a/solution.py
+++ b/solution.py
@@ -110,12 +110,29 @@
             return weights[m].at[place]
         return weights[m].at[:, pl.ds(pl.multiple_of(place * chunk, 128), chunk)]
 
-    def to_y(m, k, src):
+    units = [(m, k, 0) for m in FIRST for k in range(n_z - 1, 0, -1)]
+    units += [(m, k, 0) for m in LAST for k in (1, *range(n_z - 1, 1, -1))]
+    halved = units[-1][:2]
+    units.append((*halved, 1))
+
+    def half(ref, m, k, j):
+        if (m, k) != halved:
+            return ref
+        rows = ref.shape[0] // 2
+        return ref.at[pl.ds(j * rows, rows)]
+
+    def z_sems(m, k, j=0):
+        i = 9 * (n_z - 1) if j else m * (n_z - 1) + k - 1
+        return wz_s.at[i], wz_r.at[i]
+
+    def y_sems(m, k, j, o):
+        i = 9 * n_z if j else m * n_z + k
+        return wy_s.at[i, o - 1], wy_r.at[i, o - 1]
+
+    def to_y(m, k, src, j=0):
         for o in range(1, n_y):
-            send(
-                "weights", src, slot(m, along(k)[0]), wy_s.at[m, k, o - 1], wy_r.at[m, k, o - 1],
-                (z * n_y + (y + o) % n_y, tp),
-            )
+            dst = half(slot(m, along(k)[0]), m, k, j)
+            send("weights", src, dst, *y_sems(m, k, j, o), (z * n_y + (y + o) % n_y, tp))
 
     def tree_send(group, k, src, dst, s, r):
         for bit in bits_below(low(k) if k else n_z):
@@ -127,36 +144,36 @@
             to_y(m, 0, own)
             pltpu.make_async_copy(own, slot(m, fs), own_s.at[m]).start()
 
-    def unit_send(m, k):
-        zz = flip(z, k, n_z)
-        send("weights", part_of(m, zz), slot(m, fs), wz_s.at[m, k], wz_r.at[m, k], along(k))
-
-    def unit_forward(m, k):
-        block = slot(m, along(k)[0])
-        arrive(block, wz_s.at[m, k], wz_r.at[m, k])
-        to_y(m, k, block)
+    def unit_send(m, k, j):
+        src = half(part_of(m, flip(z, k, n_z)), m, k, j)
+        send("weights", src, half(slot(m, fs), m, k, j), *z_sems(m, k, j), along(k))
+
+    def unit_forward(m, k, j):
+        block = half(slot(m, along(k)[0]), m, k, j)
+        arrive(block, *z_sems(m, k, j))
+        to_y(m, k, block, j)
 
     def conv_start():
         for m in CONV:
-            tree_send("weights", 0, weights[m], slot(m, fs), lambda k: wz_s.at[m, k], lambda k: wz_r.at[m, k])
+            tree_send("weights", 0, weights[m], slot(m, fs), lambda k: z_sems(m, k)[0], lambda k: z_sems(m, k)[1])
         weight_own(*CONV)
 
     def conv_block(k):
         for m in CONV:
             block = slot(m, along(k)[0])
-            arrive(block, wz_s.at[m, k], wz_r.at[m, k])
-            tree_send("weights", k, block, block, lambda i: wz_s.at[m, i], lambda i: wz_r.at[m, i])
+            arrive(block, *z_sems(m, k))
+            tree_send("weights", k, block, block, lambda i: z_sems(m, i)[0], lambda i: z_sems(m, i)[1])
             to_y(m, k, block)
 
     def weight_ready(m):
         for k in range(n_z):
             zz = flip(z, k, n_z)
             for o in range(1, n_y):
-                arrive(slot(m, zz * n_y + (y + n_y - o) % n_y), wy_s.at[m, k, o - 1], wy_r.at[m, k, o - 1])
+                block = slot(m, zz * n_y + (y + n_y - o) % n_y)
+                for j in range(1 + ((m, k) == halved)):
+                    arrive(half(block, m, k, j), *y_sems(m, k, j, o))
         pltpu.make_async_copy(part_of(m, z), slot(m, fs), own_s.at[m]).wait()
 
-    units = [(m, k) for m in FIRST for k in range(n_z - 1, 0, -1)]
-    units += [(m, k) for m in LAST for k in (1, *range(n_z - 1, 1, -1))]
     sent, landed = [0], [0]
 
     def issue(count):
@@ -201,25 +218,29 @@
             arrive(dst(xx * CORES + 1 - core), c_s(xx), c_r(xx))
 
     def seq_refs(f, k):
+        b = f * n_z + k
         return (
             lambda t: xgs[f].at[k, :, columns(t)],
-            lambda i: gx_s.at[f, k, i], lambda i: gx_r.at[f, k, i],
-            lambda i: gc_s.at[f, k, i], lambda i: gc_r.at[f, k, i],
+            lambda i: gx_s.at[b, i], lambda i: gx_r.at[b, i],
+            lambda i: gc_s.at[b, i], lambda i: gc_r.at[b, i],
         )
+
+    def line_sems(f, k):
+        return gz_s.at[f * (n_z - 1) + k - 1], gz_r.at[f * (n_z - 1) + k - 1]
 
     def gather_start(f, src):
         group = ("gather", f)
         for bit in bits_below(cuts[f]):
-            send(group, src, xgs[f].at[bit, :, columns(tp)], gz_s.at[f, bit], gz_r.at[f, bit], along(bit))
+            send(group, src, xgs[f].at[bit, :, columns(tp)], *line_sems(f, bit), along(bit))
         spread(group, src, *seq_refs(f, 0))
         xgs[f][0, :, columns(tp)] = src[...]
 
     def gather_block(f, k):
         group = ("gather", f)
         block = xgs[f].at[k, :, columns(tp)]
-        arrive(block, gz_s.at[f, k], gz_r.at[f, k])
+        arrive(block, *line_sems(f, k))
         for bit in bits_below(low(k)):
-            send(group, block, xgs[f].at[k ^ bit, :, columns(tp)], gz_s.at[f, k ^ bit], gz_r.at[f, k ^ bit], along(bit))
+            send(group, block, xgs[f].at[k ^ bit, :, columns(tp)], *line_sems(f, k ^ bit), along(bit))
         spread(group, block, *seq_refs(f, k))
 
     def gather_pass(f, k):
@@ -270,16 +291,61 @@
         def give(k):
             reduce_give(
                 group, hiddens[f].at[k], down, lambda i: core_out.at[k, i], lambda i: core_in.at[k, i],
-                lambda i: rc_s.at[f, k, i], lambda i: rc_r.at[f, k, i],
+                lambda i: rc_s.at[f * n_z + k, i], lambda i: rc_r.at[f * n_z + k, i],
             )
 
         def take(k):
             reduce_take(
                 group, hiddens[f].at[k], down, lambda i: core_in.at[k, i],
-                lambda i: rc_s.at[f, k, i], lambda i: rc_r.at[f, k, i],
+                lambda i: rc_s.at[f * n_z + k, i], lambda i: rc_r.at[f * n_z + k, i],
                 lambda i: side_out.at[k, i], lambda i: side_in.at[k, i],
-                lambda i: rx_s.at[f, k, i], lambda i: rx_r.at[f, k, i], held.at[k],
+                lambda i: rx_s.at[f * n_z + k, i], lambda i: rx_r.at[f * n_z + k, i], held.at[k],
             )
+
+        def line_add(k, i):
+            arrive(line_in.at[i], rz_s.at[f * (n_z - 1)], rz_r.at[f * n_z + i])
+            held[k] = held[k] + line_in[i].astype(F32)
+
+        def line_copy(k, i, dest):
+            return remote(line_out.at[k - 1], line_in.at[i], rz_s.at[f * (n_z - 1) + k - 1], rz_r.at[f * n_z + i], along(dest))
+
+        def line_go(k, i, dest):
+            line_out[k - 1] = held[k].astype(BF16)
+            line_copy(k, i, dest).start()
+
+        def line_tree(k):
+            for bit in bits_below(low(k) if k else cuts[f]):
+                line_add(k, (k ^ bit) - 1)
+            if k:
+                line_go(k, k - 1, low(k))
+                pending.setdefault(group, []).append(line_copy(k, k - 1, low(k)))
+
+        def line_inner(k):
+            inner = (z + 1) // 2 % 2
+
+            def outer_far():
+                line_go(k, 5 - k, 1)
+
+            def inner_near():
+                line_add(2, 2)
+                line_go(2, 1, 2)
+
+            def inner_far():
+                line_add(3, 3)
+                line_go(3, 1, 3)
+
+            if k > 1:
+                pl.when(inner == 0)(outer_far)
+            if k == 2:
+                pl.when(inner == 1)(inner_near)
+            if k == 1:
+                line_go(1, 0, 1)
+                pl.when(inner == 1)(inner_far)
+            if k == 0:
+                line_add(0, 0)
+                line_add(0, 1)
+            else:
+                pending.setdefault(group, []).append(line_copy(k, 0, 1))
 
         give(cuts[f] - 1)
         for k in range(cuts[f] - 1, -1, -1):
@@ -290,17 +356,13 @@
         for k in range(cuts[f] - 1, -1, -1):
             act(plan.get(k, ()))
             reduce_sum(
-                lambda i: side_in.at[k, i], lambda i: rx_s.at[f, k, i], lambda i: rx_r.at[f, k, i], held.at[k]
+                lambda i: side_in.at[k, i], lambda i: rx_s.at[f * n_z + k, i], lambda i: rx_r.at[f * n_z + k, i], held.at[k]
             )
-            total = held[k]
-            for bit in bits_below(low(k) if k else cuts[f]):
-                i = (k ^ bit) - 1
-                arrive(line_in.at[i], rz_s.at[f, i], rz_r.at[f, i])
-                total = total + line_in[i].astype(F32)
-            if k == 0:
-                return total
-            line_out[k - 1] = total.astype(BF16)
-            send(group, line_out.at[k - 1], line_in.at[k - 1], rz_s.at[f, k - 1], rz_r.at[f, k - 1], along(low(k)))
+            if cuts[f] == 4:
+                line_inner(k)
+            else:
+                line_tree(k)
+        return held[0]
 
     def stats_start(phase, values):
         sums = jnp.sum(values, axis=-1, keepdims=True)
@@ -375,8 +437,8 @@
 
     conv_refs = (
         lambda t: xc.at[:, columns(t)],
-        lambda i: gx_s.at[2, 0, i], lambda i: gx_r.at[2, 0, i],
-        lambda i: gc_s.at[2, 0, i], lambda i: gc_r.at[2, 0, i],
+        lambda i: gx_s.at[n_z + cuts[1], i], lambda i: gx_r.at[n_z + cuts[1], i],
+        lambda i: gc_s.at[n_z + cuts[1], i], lambda i: gc_r.at[n_z + cuts[1], i],
     )
     spread("conv", out_ref, *conv_refs)
     xc[:, columns(tp)] = first
@@ -411,8 +473,8 @@
     normed = (current[:, 0:channels] - center) * scale * row_of(conv_gain)
     acted[...] = (normed * jax.nn.sigmoid(normed)).astype(BF16)
     until(5)
-    conv_core = (lambda i: rc_s.at[2, 0, i], lambda i: rc_r.at[2, 0, i])
-    conv_side = (lambda i: rx_s.at[2, 0, i], lambda i: rx_r.at[2, 0, i])
+    conv_core = (lambda i: rc_s.at[n_z + cuts[1], i], lambda i: rc_r.at[n_z + cuts[1], i])
+    conv_side = (lambda i: rx_s.at[n_z + cuts[1], i], lambda i: rx_r.at[n_z + cuts[1], i])
     reduce_give("conv", acted, bufs[5], lambda i: c_core_out.at[i], lambda i: c_core_in.at[i], *conv_core)
     issue(2)
     reduce_take(
@@ -427,7 +489,7 @@
     out_ref[...] = second
 
     gather_start(1, out_ref)
-    issue(1)
+    issue(2)
     forward(2)
     gather_block(1, 1)
     forward(1)
@@ -435,7 +497,7 @@
     until(6, 7)
     collect(*seq_refs(1, 0))
     ffn_hidden(1, 0, bufs[6], bufs[7])
-    forward(1)
+    forward(2)
     for k in range(1, cuts[1]):
         if k > 1:
             gather_block(1, k)
@@ -484,7 +546,8 @@
         proj = pltpu.VMEM((n_fs, channels, part), BF16)
         dma = pltpu.SemaphoreType.DMA
         vmem = pl.BlockSpec(memory_space=pltpu.VMEM)
-        others, others_z = max(n_x - 1, 1), max(n_z - 1, 1)
+        others = max(n_x - 1, 1)
+        blocks_in_all = n_z + cuts[1] + 1
 
         def blocks(*lead, kind=BF16):
             return pltpu.VMEM(lead + (length, width), kind)
@@ -507,8 +570,8 @@
                 blocks(n_z, others),
                 blocks(n_z, others),
                 blocks(n_z, kind=F32),
-                blocks(others_z),
-                blocks(others_z),
+                blocks(n_z),
+                blocks(n_z),
                 blocks(n_x),
                 blocks(n_x),
                 blocks(others),
@@ -518,15 +581,15 @@
                 pltpu.VMEM((length, channels), BF16),
                 pltpu.VMEM((4, n_tp, 8, length), F32),
             ]
-            + pair(9, n_z)
-            + pair(9, n_z, max(n_y - 1, 1))
+            + pair(9 * (n_z - 1) + 1)
+            + pair(9 * n_z + 1, max(n_y - 1, 1))
             + [dma((9,))]
-            + pair(2, n_z)
-            + pair(3, n_z, others)
-            + pair(3, n_z, n_x)
-            + pair(3, n_z, n_x)
-            + pair(3, n_z, others)
-            + pair(2, others_z)
+            + pair(n_z + cuts[1] - 2)
+            + pair(blocks_in_all, others)
+            + pair(blocks_in_all, n_x)
+            + pair(blocks_in_all, n_x)
+            + pair(blocks_in_all, others)
+            + [dma((n_z + cuts[1] - 2,)), dma((n_z + cuts[1] - 1,))]
             + pair(4, n_tp - 1),
             compiler_params=pltpu.CompilerParams(
                 collective_id=0, has_side_effects=True, vmem_limit_bytes=67000000

time: 260 us -> 256 us (0.985)
  Pallas kernels: 258 us -> 254 us
    pallas_call x1, Pallas kernels: 258 us -> 254 us  [body(): pl.pallas_call(functools.partial(layer_kernel, n_z, n_y, n_x, cuts), out_...]
where the time goes in v4:
time: 256 us
  Pallas kernels  254 us (99%)
    pallas_call x1, Pallas kernels, body(): pl.pallas_call(functools.partial(layer_kernel, n_z, n_y, n_x, cuts), out_...  254 us

profile of v4, /device:TPU:0, one launch (start us, length us, event | category | flops | bytes accessed | tf_op | source)
XLA Modules:
  0.0 256.0 jit_solution(17664473428276892219)
XLA Ops:
  0.0 254.2 %shard_map.145 = bf16[384,512]{1,0:T(8,128)(2,1)} custom-call(bf16[384,512]{1,0:T(8,128)(2,1)} %bitcast.3, bf16[256,1536]{1,0:T(8,128)(2,1)} %refs_0_.1, bf16[256,1536]{1,0:T(8,128)(2,1)} %refs_1_.1, bf16[1536,256]{1,0:T(8,128)(2,1)} %refs_2_.1, bf16[256,256]{1,0:T(8,128)(2,1)} %refs_3_.1, bf16[256,256]{1,0:T(8,128)(2,1)} %refs_4_.1, ...), custom_call_target="tpu_custom_call" | custom-call | tf_op jit(solution)/shard_map/pallas_call | solution.py:558
  254.3 1.8 copy.17

commit v5 on v4

--- a/solution.py
+++ b/solution.py
@@ -429,8 +429,9 @@
         "given": [(conv_block, 1), (conv_block, 2), (issue, 1)],
         2: [(forward, 1)],
         1: [(forward, 1), (weight_own, LAST[2])],
+        0: [(issue, 1)],
     })
-    issue(2)
+    issue(1)
     forward(1)
     first = post_norm(0, first_gain)
     out_ref[...] = first
@@ -444,7 +445,7 @@
     xc[:, columns(tp)] = first
     conv_block(3)
     forward(1)
-    issue(1)
+    issue(2)
     pass_on("conv", *conv_refs)
     until(3, 4)
     collect(*conv_refs)
@@ -476,7 +477,7 @@
     conv_core = (lambda i: rc_s.at[n_z + cuts[1], i], lambda i: rc_r.at[n_z + cuts[1], i])
     conv_side = (lambda i: rx_s.at[n_z + cuts[1], i], lambda i: rx_r.at[n_z + cuts[1], i])
     reduce_give("conv", acted, bufs[5], lambda i: c_core_out.at[i], lambda i: c_core_in.at[i], *conv_core)
-    issue(2)
+    issue(1)
     reduce_take(
         "conv", acted, bufs[5], lambda i: c_core_in.at[i], *conv_core,
         lambda i: c_side_out.at[i], lambda i: c_side_in.at[i], *conv_side, current,

time: 256 us -> 256 us (level)
  no operation moved by 1% of the time
where the time goes in v5:
time: 256 us; the launch traced here: 255 us
  Pallas kernels  253 us (99%)
    pallas_call x1, Pallas kernels, body(): pl.pallas_call(functools.partial(layer_kernel, n_z, n_y, n_x, cuts), out_...  253 us

profile of v5, /device:TPU:0, one launch (start us, length us, event | category | flops | bytes accessed | tf_op | source)
XLA Modules:
  0.0 255.2 jit_solution(7606703926851184902)
XLA Ops:
  0.0 253.5 %shard_map.145 = bf16[384,512]{1,0:T(8,128)(2,1)} custom-call(bf16[384,512]{1,0:T(8,128)(2,1)} %bitcast.3, bf16[256,1536]{1,0:T(8,128)(2,1)} %refs_0_.1, bf16[256,1536]{1,0:T(8,128)(2,1)} %refs_1_.1, bf16[1536,256]{1,0:T(8,128)(2,1)} %refs_2_.1, bf16[256,256]{1,0:T(8,128)(2,1)} %refs_3_.1, bf16[256,256]{1,0:T(8,128)(2,1)} %refs_4_.1, ...), custom_call_target="tpu_custom_call" | custom-call | tf_op jit(solution)/shard_map/pallas_call | solution.py:559
  253.5 1.8 copy.17
